TPU v7x, 32 devices: a whole 2x2x4 slice. The times are simulated.
32 devices in a mesh: sp: 8 (over z, x), dp: 4 (over y, core).
Axes of the slice: x: 2, y: 2, z: 4, core: 2. Of those that a mesh axis runs over, the one named last changes fastest.
Arguments:
- skip_stream_entering: bfloat16 [4, 1024, 2048], P('dp', 'sp'), may hold values from -6 to 6
- mapped_probe_matrix: bfloat16 [4, 1024, 2048], P('dp', 'sp'), may hold values from -6 to 6
- mapped_lookup_matrix: bfloat16 [4, 1024, 2048], P('dp', 'sp'), may hold values from -6 to 6
- mapped_content_matrix: bfloat16 [4, 1024, 4096], P('dp', 'sp'), may hold values from -6 to 6
- retention_preactivation: bfloat16 [4, 1024, 2048], P('dp', 'sp'), may hold values from -4 to 12
- extra_shrinkage: float32 [4, 16, 1024], P('dp', 'sp'), may hold values from -0.6932 to 0
- attention_group_scale: float32 [4096], replicated, may hold values from 0.1 to 1.9
- final_projection_matrix: bfloat16 [4096, 2048], P(None, 'dp'), may hold values from -0.09375 to 0.09375
- blender_branch_scale: float32 [2048], replicated, may hold values from 0.1 to 1.9
- specialist_prenormal_scale: float32 [2048], replicated, may hold values from 0.1 to 1.9
- specialist_switch_matrix: bfloat16 [32, 2048, 1024], P(('sp', 'dp')), may hold values from -0.125 to 0.125
- specialist_expand_matrix: bfloat16 [32, 2048, 1024], P(('sp', 'dp')), may hold values from -0.125 to 0.125
- specialist_contract_matrix: bfloat16 [32, 1024, 2048], P(('sp', 'dp')), may hold values from -0.1875 to 0.1875
- specialist_branch_scale: float32 [2048], replicated, may hold values from 0.1 to 1.9
- assigned_specialists: int32 [4, 1024, 2], P('dp', 'sp'), may hold values from 0 to 31, all different within a row; in each aligned block of 128 rows (0 to 127, 128 to 255, ..., all dimensions but the last counted through in order) at most 13 rows name the same one
- dispatcher_logits: float32 [4, 1024, 2], P('dp', 'sp'), may hold values from 0.2 to 1
Outputs:
- layer_out: bfloat16 [4, 1024, 2048], P('dp', 'sp')
Inputs may be any that keep to these rules, and one draw needn't show every extreme that they name: `assigned_specialists`: in the rows of one device no expert is named more than 13 times; in every draw some expert reaches 13 on some device.
All inputs are finite; a program needn't handle non-finite values.
Results may differ from a plain program's by a relative error of at most 0.013.
Values may be sent and summed in bfloat16 or wider, within the bound.
A program may use at most 128 MiB of HBM per device.

v0:
```python
import jax
import jax.numpy as jnp
from jax import lax
from jax.experimental import pallas as pl
from jax.experimental.pallas import tpu as pltpu
from jax.sharding import PartitionSpec as P

D = 2048
KEY_WIDTH = 128
DV = 256
TOP = 2
BLOCK = 64


epsilon = 1e-06
softness_factor = 16.0
highest = lax.Precision.HIGHEST


def rms_scale(values, gain):
    mean_square = jnp.mean(values * values, axis=-1, keepdims=True)
    return values * lax.rsqrt(mean_square + epsilon) * gain


def local_kernel(q_ref, k_ref, v_ref, g_ref, e_ref, o_ref, r_ref, u_ref):
    rows = q_ref.shape[0]
    g = g_ref[...].astype(jnp.float32)
    logs = (jnp.minimum(g, 0.0) - jnp.log(1.0 + jnp.exp(-jnp.abs(g)))) / softness_factor
    row = lax.broadcasted_iota(jnp.int32, (rows, rows), 0)
    col = lax.broadcasted_iota(jnp.int32, (rows, rows), 1)
    causal = row >= col
    extra = jnp.sum(jnp.where(causal, e_ref[0], 0.0), axis=1, keepdims=True)
    within = extra + jnp.dot(
        causal.astype(jnp.float32), logs, precision=highest, preferred_element_type=jnp.float32
    )
    middle = within[rows // 2 - 1 : rows // 2]
    end = within[rows - 1 : rows]
    q = q_ref[...].astype(jnp.float32) * KEY_WIDTH ** (-0.5)
    k = k_ref[...].astype(jnp.float32)
    v = v_ref[...]
    lifted = (q * jnp.exp(within - middle)).astype(jnp.bfloat16)
    lowered = (k * jnp.exp(middle - within)).astype(jnp.bfloat16)
    scores = lax.dot_general(
        lifted, lowered, (((1,), (1,)), ((), ())), preferred_element_type=jnp.float32
    )
    scores = jnp.where(causal, scores, 0.0).astype(jnp.bfloat16)
    o_ref[...] = jnp.dot(scores, v, preferred_element_type=jnp.float32)
    r_ref[...] = (q * jnp.exp(within)).astype(jnp.bfloat16)
    carried = (k * jnp.exp(end - within)).astype(jnp.bfloat16)
    u_ref[0] = lax.dot_general(
        v, carried, (((0,), (0,)), ((), ())), preferred_element_type=jnp.float32
    ).astype(jnp.bfloat16)


def scan_kernel(u_ref, d_ref, s_ref):
    count = u_ref.shape[0]
    decay = jnp.exp(d_ref[0])
    state = jnp.zeros(u_ref.shape[2:], jnp.float32)
    for i in range(count):
        s_ref[i, 0] = state.astype(jnp.bfloat16)
        if i < count - 1:
            state = state * decay[i : i + 1] + u_ref[i, 0].astype(jnp.float32)


def finish_kernel(o_ref, r_ref, s_ref, gain_ref, out_ref):
    mixed = o_ref[...] + lax.dot_general(
        r_ref[...], s_ref[0], (((1,), (1,)), ((), ())), preferred_element_type=jnp.float32
    )
    out_ref[...] = rms_scale(mixed, gain_ref[...]).astype(jnp.bfloat16)


def linear_attention(query, key, value, gate, extra_shrinkage, gains):
    rows, width = query.shape
    heads = width // KEY_WIDTH
    sp_count = lax.axis_size("sp")
    own = extra_shrinkage.shape[0]
    logs = jnp.sum(jax.nn.log_sigmoid(gate.astype(jnp.float32)), axis=0) / softness_factor
    spans = jnp.transpose(extra_shrinkage.reshape(own, sp_count, rows), (1, 0, 2))
    small = jnp.concatenate([spans, logs.reshape(sp_count, own, KEY_WIDTH)], axis=2)
    small = lax.all_to_all(small, "sp", split_axis=0, concat_axis=0, tiled=True)
    extra = small[:, :, :rows].reshape(heads, 1, rows)
    decays = jnp.transpose(small[:, :, rows:] + jnp.sum(spans, axis=2)[:, :, None], (1, 0, 2))
    narrow = pl.BlockSpec((rows, KEY_WIDTH), lambda h: (0, h))
    wide = pl.BlockSpec((rows, DV), lambda h: (0, h))
    state = pl.BlockSpec((1, DV, KEY_WIDTH), lambda h: (h, 0, 0))
    inside, reached, updates = pl.pallas_call(
        local_kernel,
        grid=(heads,),
        in_specs=[narrow, narrow, wide, narrow, pl.BlockSpec((1, 1, rows), lambda h: (h, 0, 0))],
        out_specs=[wide, narrow, state],
        out_shape=[
            jax.ShapeDtypeStruct((rows, heads * DV), jnp.float32),
            jax.ShapeDtypeStruct((rows, width), jnp.bfloat16),
            jax.ShapeDtypeStruct((heads, DV, KEY_WIDTH), jnp.bfloat16),
        ],
        name="local",
    )(query, key, value, gate, extra)
    gathered = lax.all_to_all(updates, "sp", split_axis=0, concat_axis=0, tiled=True)
    stack = pl.BlockSpec((sp_count, 1, DV, KEY_WIDTH), lambda h: (0, h, 0, 0))
    entering = pl.pallas_call(
        scan_kernel,
        grid=(own,),
        in_specs=[stack, pl.BlockSpec((1, sp_count, KEY_WIDTH), lambda h: (h, 0, 0))],
        out_specs=stack,
        out_shape=jax.ShapeDtypeStruct((sp_count, own, DV, KEY_WIDTH), jnp.bfloat16),
        name="scan",
    )(gathered.reshape(sp_count, own, DV, KEY_WIDTH), decays)
    entering = lax.all_to_all(
        entering.reshape(updates.shape), "sp", split_axis=0, concat_axis=0, tiled=True
    )
    return pl.pallas_call(
        finish_kernel,
        grid=(heads,),
        in_specs=[wide, narrow, state, pl.BlockSpec((1, DV), lambda h: (0, h))],
        out_specs=wide,
        out_shape=jax.ShapeDtypeStruct((rows, heads * DV), jnp.bfloat16),
        name="finish",
    )(inside, reached, entering, gains.reshape(1, heads * DV))


PLANES = 4
LANES = 128
MESH = pl.DeviceIdType.MESH


def expert_kernel(
    out_ref, gate_hbm, up_hbm, down_hbm, ret_ref, recv, res, gate_w, up_w, down_w,
    weight_sem, send_sem, recv_sem, back_sem, ret_sem,
):
    dp_count = lax.axis_size("dp")
    total, cap, segments, lanes = out_ref.shape
    per = total // PLANES
    me = lax.axis_index("sp") * dp_count + lax.axis_index("dp")
    plane, place = me // per, lax.rem(me, per)

    def where_is(peer):
        return (peer // dp_count, lax.rem(peer, dp_count))

    weights = [
        pltpu.make_async_copy(source.at[0], target, weight_sem.at[i])
        for i, (source, target) in enumerate(
            ((gate_hbm, gate_w), (up_hbm, up_w), (down_hbm, down_w))
        )
    ]
    for copy in weights:
        copy.start()
    barrier = pltpu.get_barrier_semaphore()

    @pl.loop(1, total)
    def _(i):
        peer = lax.rem(me + i, total)
        pl.semaphore_signal(barrier, inc=1, device_id=where_is(peer), device_id_type=MESH)

    pl.semaphore_wait(barrier, total - 1)

    @pl.loop(1, total)
    def _(i):
        peer = lax.rem(plane + i, PLANES) * per + lax.rem(place + i // PLANES, per)
        pltpu.make_async_remote_copy(
            src_ref=out_ref.at[peer],
            dst_ref=recv.at[me],
            send_sem=send_sem,
            recv_sem=recv_sem.at[plane],
            device_id=where_is(peer),
            device_id_type=MESH,
        ).start()

    pltpu.make_async_copy(out_ref.at[me], recv.at[me], recv_sem.at[plane]).start()
    for copy in weights:
        copy.wait()

    @pl.loop(0, PLANES)
    def _(step):
        group = lax.rem(plane + step, PLANES)
        base = group * per
        block = recv.at[pl.ds(base, per)]
        pltpu.make_async_copy(block, block, recv_sem.at[group]).wait()
        rows = block[...].reshape(per * cap, segments * lanes)
        gate_part = jnp.dot(rows, gate_w[...], preferred_element_type=jnp.float32)
        up_part = jnp.dot(rows, up_w[...], preferred_element_type=jnp.float32)
        hidden = (jax.nn.silu(gate_part) * up_part).astype(jnp.bfloat16)
        result = jnp.dot(hidden, down_w[...], preferred_element_type=jnp.float32)
        res[pl.ds(base, per)] = result.astype(jnp.bfloat16).reshape(per, cap, segments, lanes)

        @pl.loop(0, per)
        def _(j):
            peer = base + lax.rem(place + j, per)

            @pl.when(peer != me)
            def _():
                pltpu.make_async_remote_copy(
                    src_ref=res.at[peer],
                    dst_ref=ret_ref.at[me],
                    send_sem=back_sem,
                    recv_sem=ret_sem,
                    device_id=where_is(peer),
                    device_id_type=MESH,
                ).start()

            @pl.when(peer == me)
            def _():
                pltpu.make_async_copy(res.at[me], ret_ref.at[me], ret_sem).start()

    pltpu.make_async_copy(ret_ref, ret_ref, ret_sem).wait()
    sent = out_ref.at[pl.ds(0, total - 1)]
    pltpu.make_async_copy(sent, sent, send_sem).wait()
    answered = res.at[pl.ds(0, total - 1)]
    pltpu.make_async_copy(answered, answered, back_sem).wait()


def routed_experts(outgoing, gate_weight, up_weight, down_weight):
    buffer = pltpu.VMEM(outgoing.shape, jnp.bfloat16)
    weights = [pltpu.VMEM(w.shape[1:], jnp.bfloat16) for w in (gate_weight, up_weight, down_weight)]
    vmem = pl.BlockSpec(memory_space=pltpu.VMEM)
    anywhere = pl.BlockSpec(memory_space=pl.ANY)
    row_count = outgoing.shape[0] * outgoing.shape[1]
    return pl.pallas_call(
        expert_kernel,
        in_specs=[vmem, anywhere, anywhere, anywhere],
        out_specs=vmem,
        out_shape=jax.ShapeDtypeStruct(outgoing.shape, jnp.bfloat16),
        scratch_shapes=[
            buffer,
            buffer,
            *weights,
            pltpu.SemaphoreType.DMA((3,)),
            pltpu.SemaphoreType.DMA,
            pltpu.SemaphoreType.DMA((PLANES,)),
            pltpu.SemaphoreType.DMA,
            pltpu.SemaphoreType.DMA,
        ],
        compiler_params=pltpu.CompilerParams(
            collective_id=0, has_side_effects=True, vmem_limit_bytes=56 * 1024 * 1024
        ),
        cost_estimate=pl.CostEstimate(
            flops=6 * row_count * D * gate_weight.shape[2],
            bytes_accessed=6 * D * gate_weight.shape[2],
            transcendentals=0,
        ),
        name="experts",
    )(outgoing, gate_weight, up_weight, down_weight)


def shards(
    skip_stream_entering,
    mapped_probe_matrix,
    mapped_lookup_matrix,
    mapped_content_matrix,
    retention_preactivation,
    extra_shrinkage,
    attention_group_scale,
    final_projection_matrix,
    blender_branch_scale,
    specialist_prenormal_scale,
    specialist_switch_matrix,
    specialist_expand_matrix,
    specialist_contract_matrix,
    specialist_branch_scale,
    assigned_specialists,
    dispatcher_logits,
):
    tok_rows = mapped_probe_matrix.shape[1]
    sp_count = lax.axis_size("sp")
    dp_count = lax.axis_size("dp")
    flat_heads = linear_attention(
        mapped_probe_matrix[0],
        mapped_lookup_matrix[0],
        mapped_content_matrix[0],
        retention_preactivation[0],
        extra_shrinkage[0],
        attention_group_scale,
    )
    projected = jnp.dot(
        flat_heads,
        lax.all_gather(final_projection_matrix, "dp", axis=1, tiled=True),
        preferred_element_type=jnp.float32,
    ).astype(jnp.bfloat16)
    stream = skip_stream_entering[0].astype(jnp.float32)
    residual = (stream + rms_scale(projected.astype(jnp.float32), blender_branch_scale)).astype(
        jnp.bfloat16
    )
    expert_in = rms_scale(residual.astype(jnp.float32), specialist_prenormal_scale).astype(
        jnp.bfloat16
    )
    expert_total = sp_count * dp_count
    capacity = max(2, 5 * tok_rows * TOP // (3 * expert_total))
    chosen = assigned_specialists[0].reshape(-1)
    pair_total = chosen.shape[0]
    onehot = (chosen[:, None] == jnp.arange(expert_total, dtype=jnp.int32)[None, :]).astype(
        jnp.int32
    )
    ranks = jnp.sum((jnp.cumsum(onehot, axis=0) - onehot) * onehot, axis=1)
    slots = chosen * capacity + ranks
    table = jnp.full((expert_total * capacity,), pair_total, jnp.int32)
    table = table.at[slots].set(jnp.arange(pair_total, dtype=jnp.int32))
    segments = D // LANES
    padded = jnp.concatenate([expert_in, jnp.zeros((1, D), jnp.bfloat16)], axis=0)
    padded = padded.reshape(tok_rows + 1, segments, LANES)
    outgoing = padded[table // TOP].reshape(expert_total, capacity, segments, LANES)
    returned = routed_experts(
        outgoing, specialist_switch_matrix, specialist_expand_matrix, specialist_contract_matrix
    )
    flat_back = returned.reshape(expert_total * capacity, segments, LANES)
    pair_rows = flat_back[slots].reshape(tok_rows, TOP, segments, LANES)
    weights = dispatcher_logits[0]
    weights = weights / jnp.sum(weights, axis=1, keepdims=True)
    combined = jnp.sum(pair_rows.astype(jnp.float32) * weights[:, :, None, None], axis=1)
    combined = combined.reshape(tok_rows, D)
    layer_out = residual.astype(jnp.float32) + rms_scale(combined, specialist_branch_scale)
    return layer_out.astype(jnp.bfloat16)[None]


def solution(mesh):
    return jax.shard_map(
        shards,
        mesh=mesh,
        in_specs=(
            P("dp", "sp", None),
            P("dp", "sp", None),
            P("dp", "sp", None),
            P("dp", "sp", None),
            P("dp", "sp", None),
            P("dp", "sp", None),
            P(),
            P(None, "dp"),
            P(),
            P(),
            P(("sp", "dp"), None, None),
            P(("sp", "dp"), None, None),
            P(("sp", "dp"), None, None),
            P(),
            P("dp", "sp", None),
            P("dp", "sp", None),
        ),
        out_specs=P("dp", "sp", None),
        check_vma=False,
    )
```

profile of v0, /device:TPU:13, one launch (start us, length us, event | category | flops | bytes accessed | tf_op | source)
XLA Modules:
  0.0 241.7 jit_solution(15309042954803100786)
XLA Ops:
  6.5 0.0 all-gather.2.cloned.1.call-start
  6.5 0.7 all-gather.2.cloned.1.call-update
  7.3 0.3 copy-done.2
  7.6 0.7 fusion.6
  8.2 0.0 copy-done.4
  8.3 9.6 %all_to_all.15 = f32[8,2,256]{2,1,0:T(2,128)S(1)} all-to-all(f32[8,2,256]{2,1,0:T(2,128)S(1)} %pad_maximum_fusion), channel_id=1, replica_groups=mesh['sp'=8,'dp'=4] {'sp'}, dimensions={0} | all-to-all | bytes 32768 | tf_op jit(solution)/shard_map/all_to_all | solution.py:80
  17.9 0.6 fusion.20
  18.5 14.1 %local.1 = (f32[128,4096]{1,0:T(8,128)}, bf16[128,2048]{1,0:T(8,128)(2,1)}, bf16[16,256,128]{2,1,0:T(8,128)(2,1)}) custom-call(bf16[128,2048]{1,0:T(8,128)(2,1)} %bitcast.74, bf16[128,2048]{1,0:T(8,128)(2,1)} %bitcast.75, bf16[128,4096]{1,0:T(8,128)(2,1)} %bitcast.72, bf16[128,2048]{1,0:T(8,128)(2,1)} %bitcast.76, f32[16,1,128]{2,1,0:T(1,128)} %bitcast.77), custom_call_target="tpu_custom_call" | custom-call | tf_op jit(solution)/shard_map/local/pallas_call | solution.py:86
  32.6 4.7 %all-to-all-start.1 = ((bf16[16,256,128]{2,1,0:T(8,128)(2,1)}), bf16[16,256,128]{2,1,0:T(8,128)(2,1)S(1)}, u32[]{:S(2)}, u32[]{:S(2)}) async-start(bf16[16,256,128]{2,1,0:T(8,128)(2,1)} %get-tuple-element.10), calls=%async_computation.1 | async-start | bytes 2097152 | tf_op jit(solution)/shard_map/all_to_all | solution.py:98
  37.3 0.1 bitcast_reduce_fusion
  37.4 0.1 copy.35
  37.5 0.7 fusion.14.d_ref
  38.1 21.3 %all-to-all-done.1 = bf16[16,256,128]{2,1,0:T(8,128)(2,1)S(1)} async-done(((bf16[16,256,128]{2,1,0:T(8,128)(2,1)}), bf16[16,256,128]{2,1,0:T(8,128)(2,1)S(1)}, u32[]{:S(2)}, u32[]{:S(2)}) %all-to-all-start.1) | async-done | bytes 1048608 | tf_op jit(solution)/shard_map/all_to_all | solution.py:98
  59.4 1.0 copy-done
  60.4 2.1 scan.1
  62.6 7.5 %all-to-all-start.2 = ((bf16[16,256,128]{2,1,0:T(8,128)(2,1)}), bf16[16,256,128]{2,1,0:T(8,128)(2,1)S(1)}, u32[]{:S(2)}, u32[]{:S(2)}) async-start(bf16[16,256,128]{2,1,0:T(8,128)(2,1)} %bitcast.67), calls=%async_computation.2 | async-start | bytes 2097152 | tf_op jit(solution)/shard_map/all_to_all | solution.py:108
  70.0 0.0 copy-done.8
  70.0 0.1 copy.37
  70.1 0.1 eq.29
  70.3 0.1 eq.25
  70.4 0.6 reduce-window.6
  71.0 0.2 slice_reduce_fusion
  71.3 0.1 copy.36
  71.4 0.1 mul.97
  71.5 0.0 copy-done.9
  71.6 0.1 copy.40
  71.7 0.1 fusion.12
  71.8 1.4 scatter_custom_fusion
  73.2 19.9 %all-to-all-done.2.s_ref = bf16[16,256,128]{2,1,0:T(8,128)(2,1)S(1)} async-done(((bf16[16,256,128]{2,1,0:T(8,128)(2,1)}), bf16[16,256,128]{2,1,0:T(8,128)(2,1)S(1)}, u32[]{:S(2)}, u32[]{:S(2)}) %all-to-all-start.2) | async-done | bytes 1048608 | tf_op jit(solution)/shard_map/all_to_all | solution.py:108
  93.1 1.0 copy-done.1
  94.1 11.3 %finish.1 = bf16[128,4096]{1,0:T(8,128)(2,1)} custom-call(f32[128,4096]{1,0:T(8,128)} %get-tuple-element.8.o_ref, bf16[128,2048]{1,0:T(8,128)(2,1)} %get-tuple-element.9.r_ref, bf16[16,256,128]{2,1,0:T(8,128)(2,1)} %copy-done.1, f32[1,4096]{1,0:T(1,128)} %bitcast.80), custom_call_target="tpu_custom_call" | custom-call | tf_op jit(solution)/shard_map/finish/pallas_call | solution.py:111
  105.4 10.1 %all-gather.2.cloned.1.call-done = bf16[4096,2048]{1,0:T(8,128)(2,1)} async-done(((bf16[4096,512]{1,0:T(8,128)(2,1)}), bf16[4096,2048]{1,0:T(8,128)(2,1)}) %all-gather.2.cloned.1.call-update) | async-done | bytes 16777232 | tf_op jit(solution)/shard_map/all_gather | solution.py:275
  115.4 8.5 %multiply_reduce_fusion.1 = (f32[128]{0:T(128)S(1)}, f32[128,2048]{1,0:T(8,128)S(1)}) fusion(bf16[128,4096]{1,0:T(8,128)(2,1)} %finish.1, bf16[4096,2048]{1,0:T(8,128)(2,1)} %all-gather.2.cloned.1.call-done), kind=kOutput, calls=%fused_computation.21 | convolution fusion | flops 2148532224 | bytes 18874880 | tf_op jit(solution)/shard_map/dot_general | solution.py:273
  124.0 0.0 copy-start.6
  124.0 0.0 copy-done.3
  124.0 0.0 copy-done.5
  124.0 0.4 fusion.2
  124.4 0.3 copy-done.6
  124.7 0.2 fusion.4
  124.9 0.1 copy.43
  125.1 2.6 %gather_fusion = bf16[416,16,128]{2,1,0:T(8,128)(2,1)} fusion(bf16[129,16,128]{2,1,0:T(8,128)(2,1)S(1)} %slice.23, s32[1024]{0:T(1024)S(1)} %pad_clamp_fusion.1), kind=kCustom, calls=%fused_computation | custom fusion | bytes 3409536 | tf_op jit(solution)/shard_map/gather | solution.py:299
  127.7 102.1 %experts.1 = bf16[32,13,16,128]{3,2,1,0:T(8,128)(2,1)} custom-call(bf16[32,13,16,128]{3,2,1,0:T(8,128)(2,1)} %bitcast.71, bf16[1,2048,1024]{2,1,0:T(8,128)(2,1)} %gate_hbm.1, bf16[1,2048,1024]{2,1,0:T(8,128)(2,1)} %up_hbm.1, bf16[1,1024,2048]{2,1,0:T(8,128)(2,1)} %down_hbm.1), custom_call_target="tpu_custom_call" | custom-call | flops 5234491392 | bytes 12582912 | tf_op jit(solution)/shard_map/experts/pallas_call | solution.py:217
  229.8 2.3 gather_fusion.1
  232.1 0.0 copy-start.7
  232.1 0.3 fusion.1
  232.5 1.0 multiply_reduce_fusion
  233.5 0.0 copy-done.7
  233.5 1.3 fusion.9
  (26 shorter events, 0.2 us)
Async XLA Ops:
  6.5 1.0 copy-start.2
  6.5 1.7 copy-start.4
  6.5 108.9 %all-gather.2.cloned.1.call-start = ((), (), s32[]{:S(2)}) async-start(), calls=%async_computation.3 | async-start | bytes 20971520 | tf_op jit(solution)/shard_map/all_gather | solution.py:275
  32.6 26.8 %all-to-all-start.1 = ((bf16[16,256,128]{2,1,0:T(8,128)(2,1)}), bf16[16,256,128]{2,1,0:T(8,128)(2,1)S(1)}, u32[]{:S(2)}, u32[]{:S(2)}) async-start(bf16[16,256,128]{2,1,0:T(8,128)(2,1)} %get-tuple-element.10), calls=%async_computation.1 | async-start | bytes 2097152 | tf_op jit(solution)/shard_map/all_to_all | solution.py:98
  59.4 1.0 copy-start
  60.4 9.6 %copy-start.8 = (s32[1,128,2]{1,2,0:T(2,128)S(1)}, s32[1,128,2]{1,2,0:T(2,128)}, u32[]{:S(2)}) copy-start(s32[1,128,2]{1,2,0:T(2,128)} %param.30) | copy-start | bytes 3076
  60.4 11.1 %copy-start.9 = (f32[1,128,2]{1,2,0:T(2,128)S(1)}, f32[1,128,2]{1,2,0:T(2,128)}, u32[]{:S(2)}) copy-start(f32[1,128,2]{1,2,0:T(2,128)} %param.31) | copy-start | bytes 3076
  62.6 30.6 %all-to-all-start.2 = ((bf16[16,256,128]{2,1,0:T(8,128)(2,1)}), bf16[16,256,128]{2,1,0:T(8,128)(2,1)S(1)}, u32[]{:S(2)}, u32[]{:S(2)}) async-start(bf16[16,256,128]{2,1,0:T(8,128)(2,1)} %bitcast.67), calls=%async_computation.2 | async-start | bytes 2097152 | tf_op jit(solution)/shard_map/all_to_all | solution.py:108
  93.1 1.0 copy-start.1
  105.4 18.6 %copy-start.3 = (bf16[1,128,2048]{2,1,0:T(8,128)(2,1)S(1)}, bf16[1,128,2048]{2,1,0:T(8,128)(2,1)}, u32[]{:S(2)}) copy-start(bf16[1,128,2048]{2,1,0:T(8,128)(2,1)} %param.16) | copy-start | bytes 1572868
  105.4 18.6 %copy-start.5 = (f32[2048]{0:T(1024)S(1)}, f32[2048]{0:T(1024)}, u32[]{:S(2)}) copy-start(f32[2048]{0:T(1024)} %param.24) | copy-start | bytes 24580
  124.0 0.7 copy-start.6
  232.1 1.4 copy-start.7
Sparse Core Ops, SparseCore 0:
  8.9 106.4 all-gather.1
where the time goes:
time: 245 us; the launch traced here: 242 us
  Pallas kernels  130 us (53%)
  waiting for transfers between devices  51.9 us (21%)
  between operations  13.6 us (6%)
  starting transfers between devices  12.2 us (5%)
  local copies, waits for them, and re-layouts  10.7 us (4%)
  blocking collectives  9.65 us (4%)
  matrix products  8.52 us (3%)
  other arithmetic  5.51 us (2%)
    pallas_call x1, Pallas kernels, routed_experts(): pl.pallas_call(expert_kernel, in_specs=[vmem, anywhere, anywhere, anywher...  102 us
    all_to_all x1, waiting for transfers between devices, linear_attention(): lax.all_to_all(updates, 'sp', split_axis=0, concat_axis=0, tiled=True)  21.3 us
    all_to_all x1, waiting for transfers between devices, linear_attention(): lax.all_to_all(entering.reshape(updates.shape), 'sp', split_axis=0, conca...  19.9 us
    pallas_call x1, Pallas kernels, linear_attention(): pl.pallas_call(local_kernel, grid=(heads,), in_specs=[narrow, narrow, wid...  14.1 us
    pallas_call x1, Pallas kernels, linear_attention(): pl.pallas_call(finish_kernel, grid=(heads,), in_specs=[wide, narrow, stat...  11.3 us
    all_gather x1, waiting for transfers between devices, shards(): lax.all_gather(final_projection_matrix, 'dp', axis=1, tiled=True)  10.1 us
    all_to_all x1, blocking collectives, linear_attention(): small = lax.all_to_all(small, 'sp', split_axis=0, concat_axis=0, tiled=True)  9.65 us
    dot_general x1, matrix products, shards(): jnp.dot(flat_heads, lax.all_gather(final_projection_matrix, 'dp', axis=1,...  8.52 us
  transfers between devices with their start and end apart: 3, of which 3 were waited for; matrix products, arithmetic and copies ran while one was open for 2% of the time, Pallas kernels for 11%

commit v1 on v0

v1 whole, which is shorter than its diff:
```python
import functools

import jax
import jax.numpy as jnp
from jax import lax
from jax.experimental import pallas as pl
from jax.experimental.pallas import tpu as pltpu
from jax.sharding import PartitionSpec as P

D = 2048
KEY_WIDTH = 128
DV = 256
TOP = 2
BLOCK = 64


epsilon = 1e-06
softness_factor = 16.0


def rms_scale(values, gain):
    mean_square = jnp.mean(values * values, axis=-1, keepdims=True)
    return values * lax.rsqrt(mean_square + epsilon) * gain


PLANES = 4
LANES = 128
MESH = pl.DeviceIdType.MESH


def pair_rows(h, width):
    return pl.ds(pl.multiple_of(h * width, width), width)


def layer_kernel(
    q_hbm, k_hbm, v_hbm, g_hbm, stream_hbm, w_hbm, gate_hbm, up_hbm, down_hbm,
    extra_ref, gain_ref, branch_ref, pre_ref, post_ref, chosen_ref, logits_ref, out_ref,
    q_ref, k_ref, v_ref, g_ref, stream_ref, w_buf, extras, within, lifted, lowered, reached, inside,
    states_out, states, decays_out, decays, entering, onward, crossed, own_heads, peer_heads,
    proj_out, proj,
    load_sem, w_sem, extra_send, extra_recv, state_send, state_recv, decay_send, decay_recv,
    chain_send, chain_recv, cross_send, cross_recv, head_send, head_recv, proj_send, proj_recv,
    residuals, tokens, outgoing, arrivals, results, returned, combined, gate_w, up_w, down_w,
    route_rows, source_rows, slots, sources, shares,
    weight_sem, route_sem, row_send, row_recv, back_send, back_recv,
):
    sp_count, dp_count = lax.axis_size("sp"), lax.axis_size("dp")
    sp, dp = lax.axis_index("sp"), lax.axis_index("dp")
    pair, side = sp // 2, lax.rem(sp, 2)
    pairs = sp_count // 2
    y, core = dp // 2, lax.rem(dp, 2)
    ys = dp_count // 2
    rows = q_ref.shape[0]
    heads = q_ref.shape[1] // KEY_WIDTH
    half = heads // 2
    own = extra_ref.shape[0]
    cols = w_hbm.shape[1]
    partner = (sp + 1 - 2 * side, dp)
    twin = (sp, dp + 1 - 2 * core)

    def remote(src, dst, send, recv, where):
        return pltpu.make_async_remote_copy(
            src_ref=src, dst_ref=dst, send_sem=send, recv_sem=recv,
            device_id=where, device_id_type=MESH,
        )

    def peer_y(k):
        return (sp, lax.rem(y + k, ys) * 2 + core)

    loads = [
        pltpu.make_async_copy(src, dst, load_sem.at[i])
        for i, (src, dst) in enumerate(
            ((g_hbm, g_ref), (k_hbm, k_ref), (v_hbm, v_ref), (q_hbm, q_ref),
             (stream_hbm, stream_ref), (w_hbm, w_buf.at[core]))
        )
    ]
    for copy in loads:
        copy.start()

    total = sp_count * dp_count
    me = sp * dp_count + dp
    cap = outgoing.shape[1]
    per = total // PLANES
    plane, place = me // per, lax.rem(me, per)

    def where_is(peer):
        return (peer // dp_count, lax.rem(peer, dp_count))

    barrier = pltpu.get_barrier_semaphore()

    @pl.loop(1, total)
    def _(i):
        peer = lax.rem(me + i, total)
        pl.semaphore_signal(barrier, inc=1, device_id=where_is(peer), device_id_type=MESH)

    row = lax.broadcasted_iota(jnp.int32, (rows, rows), 0)
    col = lax.broadcasted_iota(jnp.int32, (rows, rows), 1)
    causal = row >= col
    ones = jnp.where(causal, 1.0, 0.0).astype(jnp.bfloat16)
    ones = jnp.concatenate([ones, ones], axis=1)

    expert = lax.broadcasted_iota(jnp.int32, (total, rows), 0)
    picks = [chosen_ref[j : j + 1] for j in range(TOP)]
    named = functools.reduce(jnp.logical_or, [expert == pick for pick in picks])
    before = jnp.dot(
        jnp.where(named, 1.0, 0.0).astype(jnp.bfloat16),
        jnp.where(row < col, 1.0, 0.0).astype(jnp.bfloat16),
        preferred_element_type=jnp.float32,
    )
    spot = lax.broadcasted_iota(jnp.int32, (rows, source_rows.shape[1]), 1).astype(jnp.float32)
    token = lax.broadcasted_iota(jnp.int32, spot.shape, 0).astype(jnp.float32)
    source = jnp.zeros(spot.shape, jnp.float32)
    for j, pick in enumerate(picks):
        rank = jnp.sum(jnp.where(expert == pick, before, 0.0), axis=0, keepdims=True)
        slot = pick.astype(jnp.float32) * cap + rank
        route_rows[j : j + 1] = pick
        route_rows[TOP + j : TOP + j + 1] = jnp.clip(rank.astype(jnp.int32), 0, cap - 1)
        upright = jnp.sum(jnp.where(row == col, slot, 0.0), axis=1, keepdims=True)
        source = source + jnp.where(spot == upright, token, 0.0)
    source = jnp.sum(source, axis=0, keepdims=True).astype(jnp.int32)
    source_rows[...] = jnp.clip(source, 0, rows - 1)
    loads[0].wait()

    @pl.loop(0, half)
    def _(j):
        cut = pair_rows(j, 2 * KEY_WIDTH)
        g = g_ref[:, cut].astype(jnp.float32)
        logs = (jnp.minimum(g, 0.0) - jnp.log(1.0 + jnp.exp(-jnp.abs(g)))) / softness_factor
        high = logs.astype(jnp.bfloat16)
        low = (logs - high.astype(jnp.float32)).astype(jnp.bfloat16)
        within[:, cut] = jnp.dot(
            ones, jnp.concatenate([high, low], axis=0), preferred_element_type=jnp.float32
        )

    tables = [
        pltpu.make_async_copy(src, dst, route_sem.at[i])
        for i, (src, dst) in enumerate(
            ((route_rows, slots), (source_rows, sources), (logits_ref, shares))
        )
    ]
    for copy in tables:
        copy.start()
    pl.semaphore_wait(barrier, total - 1)

    @pl.loop(1, sp_count)
    def _(i):
        peer = lax.rem(sp + i, sp_count)
        remote(
            extra_ref.at[:, pair_rows(peer, rows)], extras.at[sp], extra_send, extra_recv, (peer, dp)
        ).start()

    pltpu.make_async_copy(
        extra_ref.at[:, pair_rows(sp, rows)], extras.at[sp], extra_recv
    ).start()
    w_copy = remote(w_hbm, w_buf.at[core], w_sem.at[0], w_sem.at[1], twin)
    w_copy.start()

    @pl.when(pair == 0)
    def _():
        entering[0] = jnp.zeros(entering.shape[1:], entering.dtype)

    for copy in loads[1:4]:
        copy.wait()
    weights = [
        pltpu.make_async_copy(src.at[0], dst, weight_sem.at[i])
        for i, (src, dst) in enumerate(
            ((gate_hbm, gate_w), (up_hbm, up_w), (down_hbm, down_w))
        )
    ]
    for copy in weights:
        copy.start()
    pltpu.make_async_copy(extras, extras, extra_recv).wait()

    def local_state(h):
        cut = pair_rows(h, KEY_WIDTH)
        extra = jnp.sum(
            jnp.where(causal, extras[h // own, pl.ds(lax.rem(h, own), 1)], 0.0),
            axis=1, keepdims=True,
        )
        b = within[:, cut] + extra
        middle = b[rows // 2 - 1 : rows // 2]
        end = b[rows - 1 : rows]
        up = jnp.exp(b - middle)
        down = jnp.exp(middle - b)
        q = q_ref[:, cut].astype(jnp.float32) * (KEY_WIDTH ** (-0.5)) * up
        k = k_ref[:, cut].astype(jnp.float32) * down
        lifted[:, cut] = q.astype(jnp.bfloat16)
        lowered[:, cut] = k.astype(jnp.bfloat16)
        reached[:, cut] = (q * jnp.exp(middle)).astype(jnp.bfloat16)
        carried = (k * jnp.exp(end - middle)).astype(jnp.bfloat16)
        state = lax.dot_general(
            v_ref[:, pair_rows(h, DV)], carried, (((0,), (0,)), ((), ())),
            preferred_element_type=jnp.float32,
        )
        return state.astype(jnp.bfloat16), jnp.exp(end)

    @pl.loop(0, half // 2)
    def _(j):
        for i in (2 * j, 2 * j + 1):
            state, decay = local_state((1 - side) * half + i)
            states_out[i] = state
            decays_out[i] = decay
        for i in (2 * j, 2 * j + 1):
            remote(
                states_out.at[i], states.at[side, i], state_send, state_recv.at[i], partner
            ).start()

    decay_copy = remote(decays_out, decays.at[side], decay_send, decay_recv, partner)
    decay_copy.start()

    @pl.loop(0, half // 2)
    def _(j):
        for i in (2 * j, 2 * j + 1):
            state, decay = local_state(side * half + i)
            states[side, i] = state
            decays[side, i] = decay

    @pl.loop(0, half)
    def _(j):
        for h in (2 * j, 2 * j + 1):
            cut = pair_rows(h, KEY_WIDTH)
            wide = pair_rows(h, DV)
            scores = lax.dot_general(
                lifted[:, cut], lowered[:, cut], (((1,), (1,)), ((), ())),
                preferred_element_type=jnp.float32,
            )
            scores = jnp.where(causal, scores, 0.0).astype(jnp.bfloat16)
            inside[:, wide] = jnp.dot(scores, v_ref[:, wide], preferred_element_type=jnp.float32)

    def finish(h, state):
        wide = pair_rows(h, DV)
        mixed = inside[:, wide] + lax.dot_general(
            reached[:, pair_rows(h, KEY_WIDTH)], state, (((1,), (1,)), ((), ())),
            preferred_element_type=jnp.float32,
        )
        own_heads[h] = rms_scale(mixed, gain_ref[:, wide]).astype(jnp.bfloat16)
        for k in range(1, ys):
            remote(
                own_heads.at[h], peer_heads.at[k - 1, h],
                head_send.at[k - 1], head_recv.at[k - 1, h], peer_y(k),
            ).start()

    def finish_crossed(i):
        pltpu.make_async_copy(crossed.at[i], crossed.at[i], cross_recv.at[i]).wait()
        finish((1 - side) * half + i, crossed[i])

    lag = 2
    remote(decays_out, decays.at[side], decay_send, decay_recv, partner).wait_recv()

    @pl.loop(0, half)
    def _(i):
        pltpu.make_async_copy(
            states_out.at[i], states_out.at[i], state_recv.at[i]
        ).wait()

        @pl.when(pair > 0)
        def _():
            pltpu.make_async_copy(onward.at[i], onward.at[i], chain_recv.at[i]).wait()

        middle = entering[0, i].astype(jnp.float32) * decays[0, i] + states[0, i].astype(jnp.float32)
        entering[1, i] = middle.astype(jnp.bfloat16)
        onward[i] = (middle * decays[1, i] + states[1, i].astype(jnp.float32)).astype(jnp.bfloat16)

        @pl.when(pair < pairs - 1)
        def _():
            remote(
                onward.at[i], entering.at[0, i], chain_send, chain_recv.at[i], (sp + 2, dp)
            ).start()

        remote(
            entering.at[1 - side, i], crossed.at[i], cross_send, cross_recv.at[i], partner
        ).start()
        finish(side * half + i, entering[side, i])

        @pl.when(i >= lag)
        def _():
            finish_crossed(i - lag)

    @pl.loop(half - lag, half)
    def _(i):
        finish_crossed(i)

    loads[5].wait()
    w_copy.wait_recv()

    def project(head_of, ready):
        total = None
        for h in range(heads):
            ready(h)
            wide = pl.ds(h * DV, DV)
            part = [
                jnp.dot(head_of(h), w_buf[c, wide, :], preferred_element_type=jnp.float32)
                for c in range(2)
            ]
            total = part if total is None else [a + b for a, b in zip(total, part)]
        return jnp.concatenate(total, axis=1).astype(jnp.bfloat16)

    for k in range(1, ys):
        def ready(h, k=k):
            pltpu.make_async_copy(
                peer_heads.at[k - 1, h], peer_heads.at[k - 1, h], head_recv.at[k - 1, h]
            ).wait()

        proj_out[k - 1] = project(lambda h, k=k: peer_heads[k - 1, h], ready)
        back = (sp, lax.rem(y - k + ys, ys) * 2 + core)
        remote(proj_out.at[k - 1], proj.at[y], proj_send, proj_recv, back).start()
    proj[y] = project(lambda h: own_heads[h], lambda h: None)
    loads[4].wait()
    arrived = proj.at[pl.ds(0, ys - 1)]
    pltpu.make_async_copy(arrived, arrived, proj_recv).wait()
    projected = jnp.concatenate([proj[i] for i in range(ys)], axis=1).astype(jnp.float32)
    residual = stream_ref[...].astype(jnp.float32) + rms_scale(projected, branch_ref[...])
    residual = residual.astype(jnp.bfloat16)
    residuals[...] = residual
    inputs = rms_scale(residual.astype(jnp.float32), pre_ref[...]).astype(jnp.bfloat16)
    segments = D // LANES
    tokens[...] = inputs.reshape(rows, segments, LANES)
    for copy in tables:
        copy.wait()

    def group_of(step):
        across = lax.rem(plane + step // 2 * 2, PLANES)
        return across + lax.rem(step, 2) * (1 - 2 * lax.rem(across, 2))

    def block(ref, peer):
        return ref.at[peer]

    @pl.loop(0, total)
    def _(i):
        group = group_of(lax.rem(i // per + 2, PLANES))
        peer = group * per + lax.rem(place + lax.rem(i, per), per)
        for r in range(cap):
            outgoing[peer, r] = tokens[jnp.clip(sources[0, peer * cap + r], 0, rows - 1)]

        @pl.when(peer != me)
        def _():
            remote(
                block(outgoing, peer), block(arrivals, me), row_send, row_recv.at[plane],
                where_is(peer),
            ).start()

        @pl.when(peer == me)
        def _():
            pltpu.make_async_copy(
                block(outgoing, me), block(arrivals, me), row_recv.at[plane]
            ).start()

    for copy in weights:
        copy.wait()

    @pl.loop(0, PLANES)
    def _(step):
        group = group_of(step)
        base = group * per
        batch = pl.ds(base, per)
        pltpu.make_async_copy(arrivals.at[batch], arrivals.at[batch], row_recv.at[group]).wait()
        x = arrivals[batch].reshape(per * cap, D)
        gate_part = jnp.dot(x, gate_w[...], preferred_element_type=jnp.float32)
        up_part = jnp.dot(x, up_w[...], preferred_element_type=jnp.float32)
        hidden = (jax.nn.silu(gate_part) * up_part).astype(jnp.bfloat16)
        result = jnp.dot(hidden, down_w[...], preferred_element_type=jnp.float32)
        results[batch] = result.astype(jnp.bfloat16).reshape(per, cap, segments, LANES)

        @pl.loop(0, per)
        def _(j):
            peer = base + lax.rem(place + j, per)

            @pl.when(peer != me)
            def _():
                remote(
                    block(results, peer), block(returned, me), back_send, back_recv,
                    where_is(peer),
                ).start()

            @pl.when(peer == me)
            def _():
                pltpu.make_async_copy(
                    block(results, me), block(returned, me), back_recv
                ).start()

    pltpu.make_async_copy(returned, returned, back_recv).wait()

    @pl.loop(0, rows // 8)
    def _(i):
        for t in range(8):
            at = i * 8 + t
            first, second = shares[0, at], shares[1, at]
            both = first + second
            rows_of = [
                returned[
                    jnp.clip(slots[j, at], 0, total - 1), jnp.clip(slots[TOP + j, at], 0, cap - 1)
                ].astype(jnp.float32)
                for j in range(TOP)
            ]
            combined[at] = rows_of[0] * (first / both) + rows_of[1] * (second / both)

    routed = rms_scale(combined[...].reshape(rows, D), post_ref[...])
    out_ref[...] = (residuals[...].astype(jnp.float32) + routed).astype(jnp.bfloat16)

    others = pl.ds(0, total - 1)
    pltpu.make_async_copy(outgoing.at[others], outgoing.at[others], row_send).wait()
    pltpu.make_async_copy(results.at[others], results.at[others], back_send).wait()

    sent = extras.at[pl.ds(0, sp_count - 1)]
    pltpu.make_async_copy(sent, sent, extra_send).wait()
    pltpu.make_async_copy(states_out, states_out, state_send).wait()
    decay_copy.wait_send()
    w_copy.wait_send()
    pltpu.make_async_copy(crossed, crossed, cross_send).wait()

    @pl.when(pair < pairs - 1)
    def _():
        pltpu.make_async_copy(onward, onward, chain_send).wait()

    for k in range(1, ys):
        pltpu.make_async_copy(own_heads, own_heads, head_send.at[k - 1]).wait()
    pltpu.make_async_copy(proj_out, proj_out, proj_send).wait()


def layer(
    query, key, value, gate, stream, weight, gate_weight, up_weight, down_weight,
    extra, gain, branch_gain, pre_gain, post_gain, chosen, logits,
):
    rows, width = query.shape
    heads = width // KEY_WIDTH
    half = heads // 2
    sp_count, dp_count = lax.axis_size("sp"), lax.axis_size("dp")
    ys = dp_count // 2
    total = sp_count * dp_count
    cols = weight.shape[1]
    cap = max(2, 5 * rows * TOP // (3 * total))
    bf16, f32, i32 = jnp.bfloat16, jnp.float32, jnp.int32
    vmem = pl.BlockSpec(memory_space=pltpu.VMEM)
    anywhere = pl.BlockSpec(memory_space=pl.ANY)
    state = (DV, KEY_WIDTH)
    table = (1, -(-total * cap // LANES) * LANES)
    units = pltpu.VMEM((total, cap, D // LANES, LANES), bf16)
    dma = pltpu.SemaphoreType.DMA
    return pl.pallas_call(
        layer_kernel,
        in_specs=[anywhere] * 9 + [vmem] * 7,
        out_specs=vmem,
        out_shape=jax.ShapeDtypeStruct((rows, D), bf16),
        scratch_shapes=[
            pltpu.VMEM((rows, width), bf16),
            pltpu.VMEM((rows, width), bf16),
            pltpu.VMEM(value.shape, bf16),
            pltpu.VMEM((rows, width), bf16),
            pltpu.VMEM((rows, D), bf16),
            pltpu.VMEM((2,) + weight.shape, bf16),
            pltpu.VMEM((sp_count, extra.shape[0], rows), f32),
            pltpu.VMEM((rows, width), f32),
            pltpu.VMEM((rows, width), bf16),
            pltpu.VMEM((rows, width), bf16),
            pltpu.VMEM((rows, width), bf16),
            pltpu.VMEM(value.shape, f32),
            pltpu.VMEM((half,) + state, bf16),
            pltpu.VMEM((2, half) + state, bf16),
            pltpu.VMEM((half, 1, KEY_WIDTH), f32),
            pltpu.VMEM((2, half, 1, KEY_WIDTH), f32),
            pltpu.VMEM((2, half) + state, bf16),
            pltpu.VMEM((half,) + state, bf16),
            pltpu.VMEM((half,) + state, bf16),
            pltpu.VMEM((heads, rows, DV), bf16),
            pltpu.VMEM((ys - 1, heads, rows, DV), bf16),
            pltpu.VMEM((ys - 1, rows, 2 * cols), bf16),
            pltpu.VMEM((ys, rows, 2 * cols), bf16),
            dma((6,)), dma((2,)), dma, dma, dma, dma((half,)), dma, dma,
            dma, dma((half,)), dma, dma((half,)), dma((ys - 1,)), dma((ys - 1, heads)), dma, dma,
            pltpu.VMEM((rows, D), bf16),
            pltpu.VMEM((rows, D // LANES, LANES), bf16),
            units, units, units, units,
            pltpu.VMEM((rows, D // LANES, LANES), f32),
            *[pltpu.VMEM(w.shape[1:], bf16) for w in (gate_weight, up_weight, down_weight)],
            pltpu.VMEM((2 * TOP, rows), i32),
            pltpu.VMEM(table, i32),
            pltpu.SMEM((2 * TOP, rows), i32),
            pltpu.SMEM(table, i32),
            pltpu.SMEM((TOP, rows), f32),
            dma((3,)), dma((3,)), dma, dma((PLANES,)), dma, dma,
        ],
        compiler_params=pltpu.CompilerParams(
            collective_id=0, has_side_effects=True, vmem_limit_bytes=60 * 1024 * 1024
        ),
        name="layer",
    )(
        query, key, value, gate, stream, weight, gate_weight, up_weight, down_weight,
        extra, gain.reshape(1, -1), branch_gain.reshape(1, -1), pre_gain.reshape(1, -1),
        post_gain.reshape(1, -1), chosen, logits,
    )


def shards(
    skip_stream_entering,
    mapped_probe_matrix,
    mapped_lookup_matrix,
    mapped_content_matrix,
    retention_preactivation,
    extra_shrinkage,
    attention_group_scale,
    final_projection_matrix,
    blender_branch_scale,
    specialist_prenormal_scale,
    specialist_switch_matrix,
    specialist_expand_matrix,
    specialist_contract_matrix,
    specialist_branch_scale,
    assigned_specialists,
    dispatcher_logits,
):
    out = layer(
        mapped_probe_matrix[0],
        mapped_lookup_matrix[0],
        mapped_content_matrix[0],
        retention_preactivation[0],
        skip_stream_entering[0],
        final_projection_matrix,
        specialist_switch_matrix,
        specialist_expand_matrix,
        specialist_contract_matrix,
        extra_shrinkage[0],
        attention_group_scale,
        blender_branch_scale,
        specialist_prenormal_scale,
        specialist_branch_scale,
        jnp.transpose(assigned_specialists[0]),
        jnp.transpose(dispatcher_logits[0]),
    )
    return out[None]


def solution(mesh):
    return jax.shard_map(
        shards,
        mesh=mesh,
        in_specs=(
            P("dp", "sp", None),
            P("dp", "sp", None),
            P("dp", "sp", None),
            P("dp", "sp", None),
            P("dp", "sp", None),
            P("dp", "sp", None),
            P(),
            P(None, "dp"),
            P(),
            P(),
            P(("sp", "dp"), None, None),
            P(("sp", "dp"), None, None),
            P(("sp", "dp"), None, None),
            P(),
            P("dp", "sp", None),
            P("dp", "sp", None),
        ),
        out_specs=P("dp", "sp", None),
        check_vma=False,
    )
```

time: 245 us -> 140 us (0.57); the launches traced: 242 us -> 140 us
  waiting for transfers between devices: 51.9 us -> 0 us
  between operations: 13.6 us -> 0.01 us
  starting transfers between devices: 12.2 us -> 0 us
  blocking collectives: 9.65 us -> 0 us
  local copies, waits for them, and re-layouts: 10.7 us -> 1.88 us
  matrix products: 8.52 us -> 0 us
  Pallas kernels: 130 us -> 138 us
  other arithmetic: 5.51 us -> 0 us
    all_to_all x2 -> x0, waiting for transfers between devices: 41.2 us -> none  [the longest x1 21.3 us: linear_attention(): lax.all_to_all(updates, 'sp', split_axis=0, concat_axis=0, tiled=True)]
    all_to_all x2 -> x0, starting transfers between devices: 12.2 us -> none  [the longest x1 7.47 us: linear_attention(): lax.all_to_all(entering.reshape(updates.shape), 'sp', split_axis=0, conca...]
    all_gather x1 -> x0, waiting for transfers between devices: 10.1 us -> none  [shards(): lax.all_gather(final_projection_matrix, 'dp', axis=1, tiled=True)]
    all_to_all x1 -> x0, blocking collectives: 9.65 us -> none  [linear_attention(): small = lax.all_to_all(small, 'sp', split_axis=0, concat_axis=0, tiled=True)]
    dot_general x1 -> x0, matrix products: 8.52 us -> none  [shards(): jnp.dot(flat_heads, lax.all_gather(final_projection_matrix, 'dp', axis=1,...]
    pallas_call x4 -> x1, Pallas kernels: 130 us -> 138 us  [layer(): pl.pallas_call(layer_kernel, in_specs=[anywhere] * 9 + [vmem] * 7, out_sp...]
    gather x2 -> x0, local copies, waits for them, and re-layouts: 4.89 us -> none  [the longest x1 2.6 us: shards(): padded[table // TOP].reshape(expert_total, capacity, segments, LANES)]
    reduce_sum x7 -> x0, other arithmetic: 2.6 us -> none  [the longest x2 1.41 us: rms_scale(): mean_square = jnp.mean(values * values, axis=-1, keepdims=True)]
  transfers between devices with their start and end apart: 3 -> 0, of which waited for: 3 -> 0; matrix products, arithmetic and copies ran while one was open for 2% -> 0% of each run, Pallas kernels for 11% -> 0%
where the time goes in v1:
time: 140 us
  Pallas kernels  138 us (99%)
  local copies, waits for them, and re-layouts  1.88 us (1%)
    pallas_call x1, Pallas kernels, layer(): pl.pallas_call(layer_kernel, in_specs=[anywhere] * 9 + [vmem] * 7, out_sp...  138 us

profile of v1, /device:TPU:13, one launch (start us, length us, event | category | flops | bytes accessed | tf_op | source)
XLA Modules:
  0.0 139.7 jit_solution(12199214505974139261)
XLA Ops:
  0.0 137.8 %layer.1 = bf16[128,2048]{1,0:T(8,128)(2,1)} custom-call(bf16[128,2048]{1,0:T(8,128)(2,1)} %bitcast.19, bf16[128,2048]{1,0:T(8,128)(2,1)} %bitcast.20, bf16[128,4096]{1,0:T(8,128)(2,1)} %bitcast.18, bf16[128,2048]{1,0:T(8,128)(2,1)} %bitcast.21, bf16[128,2048]{1,0:T(8,128)(2,1)} %bitcast.22, bf16[4096,512]{1,0:T(8,128)(2,1)} %w_hbm.1, ...), custom_call_target="tpu_custom_call" | custom-call | tf_op jit(solution)/shard_map/layer/pallas_call | solution.py:439
  137.8 1.9 %copy.18 = bf16[1,128,2048]{2,1,0:T(8,128)(2,1)} copy(bf16[1,128,2048]{2,1,0:T(8,128)(2,1)} %bitcast.17) | data formatting | bytes 1048576

commit v2 on v1

--- a/solution.py
+++ b/solution.py
@@ -41,7 +41,7 @@
     load_sem, w_sem, extra_send, extra_recv, state_send, state_recv, decay_send, decay_recv,
     chain_send, chain_recv, cross_send, cross_recv, head_send, head_recv, proj_send, proj_recv,
     residuals, tokens, outgoing, arrivals, results, returned, combined, gate_w, up_w, down_w,
-    route_rows, source_rows, slots, sources, shares,
+    route_rows, source_rows, share_rows, slots, sources, shares,
     weight_sem, route_sem, row_send, row_recv, back_send, back_recv,
 ):
     sp_count, dp_count = lax.axis_size("sp"), lax.axis_size("dp")
@@ -132,10 +132,13 @@
             ones, jnp.concatenate([high, low], axis=0), preferred_element_type=jnp.float32
         )
 
+    logits = [logits_ref[j : j + 1] for j in range(TOP)]
+    for j in range(TOP):
+        share_rows[j : j + 1] = logits[j] / sum(logits)
     tables = [
         pltpu.make_async_copy(src, dst, route_sem.at[i])
         for i, (src, dst) in enumerate(
-            ((route_rows, slots), (source_rows, sources), (logits_ref, shares))
+            ((route_rows, slots), (source_rows, sources), (share_rows, shares))
         )
     ]
     for copy in tables:
@@ -202,11 +205,11 @@
             decays_out[i] = decay
         for i in (2 * j, 2 * j + 1):
             remote(
+                decays_out.at[i], decays.at[side, i], decay_send, decay_recv.at[i], partner
+            ).start()
+            remote(
                 states_out.at[i], states.at[side, i], state_send, state_recv.at[i], partner
             ).start()
-
-    decay_copy = remote(decays_out, decays.at[side], decay_send, decay_recv, partner)
-    decay_copy.start()
 
     @pl.loop(0, half // 2)
     def _(j):
@@ -244,14 +247,12 @@
         pltpu.make_async_copy(crossed.at[i], crossed.at[i], cross_recv.at[i]).wait()
         finish((1 - side) * half + i, crossed[i])
 
-    lag = 2
-    remote(decays_out, decays.at[side], decay_send, decay_recv, partner).wait_recv()
+    lag = jnp.maximum(3, half - 2 * pair)
 
     @pl.loop(0, half)
     def _(i):
-        pltpu.make_async_copy(
-            states_out.at[i], states_out.at[i], state_recv.at[i]
-        ).wait()
+        pltpu.make_async_copy(decays_out.at[i], decays_out.at[i], decay_recv.at[i]).wait()
+        pltpu.make_async_copy(states_out.at[i], states_out.at[i], state_recv.at[i]).wait()
 
         @pl.when(pair > 0)
         def _():
@@ -384,15 +385,13 @@
     def _(i):
         for t in range(8):
             at = i * 8 + t
-            first, second = shares[0, at], shares[1, at]
-            both = first + second
             rows_of = [
                 returned[
                     jnp.clip(slots[j, at], 0, total - 1), jnp.clip(slots[TOP + j, at], 0, cap - 1)
                 ].astype(jnp.float32)
                 for j in range(TOP)
             ]
-            combined[at] = rows_of[0] * (first / both) + rows_of[1] * (second / both)
+            combined[at] = rows_of[0] * shares[0, at] + rows_of[1] * shares[1, at]
 
     routed = rms_scale(combined[...].reshape(rows, D), post_ref[...])
     out_ref[...] = (residuals[...].astype(jnp.float32) + routed).astype(jnp.bfloat16)
@@ -404,7 +403,7 @@
     sent = extras.at[pl.ds(0, sp_count - 1)]
     pltpu.make_async_copy(sent, sent, extra_send).wait()
     pltpu.make_async_copy(states_out, states_out, state_send).wait()
-    decay_copy.wait_send()
+    pltpu.make_async_copy(decays_out, decays_out, decay_send).wait()
     w_copy.wait_send()
     pltpu.make_async_copy(crossed, crossed, cross_send).wait()
 
@@ -465,7 +464,7 @@
             pltpu.VMEM((ys - 1, heads, rows, DV), bf16),
             pltpu.VMEM((ys - 1, rows, 2 * cols), bf16),
             pltpu.VMEM((ys, rows, 2 * cols), bf16),
-            dma((6,)), dma((2,)), dma, dma, dma, dma((half,)), dma, dma,
+            dma((6,)), dma((2,)), dma, dma, dma, dma((half,)), dma, dma((half,)),
             dma, dma((half,)), dma, dma((half,)), dma((ys - 1,)), dma((ys - 1, heads)), dma, dma,
             pltpu.VMEM((rows, D), bf16),
             pltpu.VMEM((rows, D // LANES, LANES), bf16),
@@ -474,6 +473,7 @@
             *[pltpu.VMEM(w.shape[1:], bf16) for w in (gate_weight, up_weight, down_weight)],
             pltpu.VMEM((2 * TOP, rows), i32),
             pltpu.VMEM(table, i32),
+            pltpu.VMEM((TOP, rows), f32),
             pltpu.SMEM((2 * TOP, rows), i32),
             pltpu.SMEM(table, i32),
             pltpu.SMEM((TOP, rows), f32),

time: 140 us -> 134 us (0.957)
  Pallas kernels: 138 us -> 132 us
    pallas_call x1, Pallas kernels: 138 us -> 132 us  [layer(): pl.pallas_call(layer_kernel, in_specs=[anywhere] * 9 + [vmem] * 7, out_sp...]
where the time goes in v2:
time: 134 us
  Pallas kernels  132 us (99%)
  local copies, waits for them, and re-layouts  1.88 us (1%)
    pallas_call x1, Pallas kernels, layer(): pl.pallas_call(layer_kernel, in_specs=[anywhere] * 9 + [vmem] * 7, out_sp...  132 us

profile of v2, /device:TPU:13, one launch (start us, length us, event | category | flops | bytes accessed | tf_op | source)
XLA Modules:
  0.0 133.7 jit_solution(18418453135184492376)
XLA Ops:
  0.0 131.9 %layer.1 = bf16[128,2048]{1,0:T(8,128)(2,1)} custom-call(bf16[128,2048]{1,0:T(8,128)(2,1)} %bitcast.19, bf16[128,2048]{1,0:T(8,128)(2,1)} %bitcast.20, bf16[128,4096]{1,0:T(8,128)(2,1)} %bitcast.18, bf16[128,2048]{1,0:T(8,128)(2,1)} %bitcast.21, bf16[128,2048]{1,0:T(8,128)(2,1)} %bitcast.22, bf16[4096,512]{1,0:T(8,128)(2,1)} %w_hbm.1, ...), custom_call_target="tpu_custom_call" | custom-call | tf_op jit(solution)/shard_map/layer/pallas_call | solution.py:438
  131.9 1.9 %copy.18 = bf16[1,128,2048]{2,1,0:T(8,128)(2,1)} copy(bf16[1,128,2048]{2,1,0:T(8,128)(2,1)} %bitcast.17) | data formatting | bytes 1048576

commit v3 on v2

--- a/solution.py
+++ b/solution.py
@@ -23,7 +23,7 @@
     return values * lax.rsqrt(mean_square + epsilon) * gain
 
 
-PLANES = 4
+CHUNKS = 4
 LANES = 128
 MESH = pl.DeviceIdType.MESH
 
@@ -40,9 +40,11 @@
     proj_out, proj,
     load_sem, w_sem, extra_send, extra_recv, state_send, state_recv, decay_send, decay_recv,
     chain_send, chain_recv, cross_send, cross_recv, head_send, head_recv, proj_send, proj_recv,
-    residuals, tokens, outgoing, arrivals, results, returned, combined, gate_w, up_w, down_w,
+    residuals, tokens, far_tokens, outgoing, arrivals, results, returned, sums_out, sums_in, combined,
+    gate_w, up_w, down_w, far_chosen, far_logits,
     route_rows, source_rows, share_rows, slots, sources, shares,
-    weight_sem, route_sem, row_send, row_recv, back_send, back_recv,
+    weight_sem, route_sem, far_send, far_recv, token_send, token_recv, row_send, row_recv,
+    back_send, back_recv, sum_send, sum_recv,
 ):
     sp_count, dp_count = lax.axis_size("sp"), lax.axis_size("dp")
     sp, dp = lax.axis_index("sp"), lax.axis_index("dp")
@@ -79,9 +81,11 @@
 
     total = sp_count * dp_count
     me = sp * dp_count + dp
-    cap = outgoing.shape[1]
-    per = total // PLANES
-    plane, place = me // per, lax.rem(me, per)
+    cap = outgoing.shape[3]
+    near = total // 2
+    per = near // 2
+    side_half, place = me // near, lax.rem(me, near)
+    mirror = lax.rem(me + near, total)
 
     def where_is(peer):
         return (peer // dp_count, lax.rem(peer, dp_count))
@@ -99,26 +103,32 @@
     ones = jnp.where(causal, 1.0, 0.0).astype(jnp.bfloat16)
     ones = jnp.concatenate([ones, ones], axis=1)
 
-    expert = lax.broadcasted_iota(jnp.int32, (total, rows), 0)
-    picks = [chosen_ref[j : j + 1] for j in range(TOP)]
-    named = functools.reduce(jnp.logical_or, [expert == pick for pick in picks])
-    before = jnp.dot(
-        jnp.where(named, 1.0, 0.0).astype(jnp.bfloat16),
-        jnp.where(row < col, 1.0, 0.0).astype(jnp.bfloat16),
-        preferred_element_type=jnp.float32,
-    )
-    spot = lax.broadcasted_iota(jnp.int32, (rows, source_rows.shape[1]), 1).astype(jnp.float32)
-    token = lax.broadcasted_iota(jnp.int32, spot.shape, 0).astype(jnp.float32)
-    source = jnp.zeros(spot.shape, jnp.float32)
-    for j, pick in enumerate(picks):
-        rank = jnp.sum(jnp.where(expert == pick, before, 0.0), axis=0, keepdims=True)
-        slot = pick.astype(jnp.float32) * cap + rank
-        route_rows[j : j + 1] = pick
-        route_rows[TOP + j : TOP + j + 1] = jnp.clip(rank.astype(jnp.int32), 0, cap - 1)
-        upright = jnp.sum(jnp.where(row == col, slot, 0.0), axis=1, keepdims=True)
-        source = source + jnp.where(spot == upright, token, 0.0)
-    source = jnp.sum(source, axis=0, keepdims=True).astype(jnp.int32)
-    source_rows[...] = jnp.clip(source, 0, rows - 1)
+    def build_tables(t, picked, scores):
+        expert = lax.broadcasted_iota(jnp.int32, (near, rows), 0)
+        picks = [picked[j : j + 1] - side_half * near for j in range(TOP)]
+        named = functools.reduce(jnp.logical_or, [expert == pick for pick in picks])
+        before = jnp.dot(
+            jnp.where(named, 1.0, 0.0).astype(jnp.bfloat16),
+            jnp.where(row < col, 1.0, 0.0).astype(jnp.bfloat16),
+            preferred_element_type=jnp.float32,
+        )
+        spot = lax.broadcasted_iota(jnp.int32, (rows, source_rows.shape[2]), 1).astype(jnp.float32)
+        token = lax.broadcasted_iota(jnp.int32, spot.shape, 0).astype(jnp.float32)
+        source = jnp.zeros(spot.shape, jnp.float32)
+        score = sum(scores[j : j + 1] for j in range(TOP))
+        for j, pick in enumerate(picks):
+            here = jnp.logical_and(pick >= 0, pick < near)
+            rank = jnp.sum(jnp.where(expert == pick, before, 0.0), axis=0, keepdims=True)
+            slot = jnp.where(here, pick.astype(jnp.float32) * cap + rank, -1.0)
+            route_rows[t, j : j + 1] = jnp.clip(pick, 0, near - 1)
+            route_rows[t, TOP + j : TOP + j + 1] = jnp.clip(rank.astype(jnp.int32), 0, cap - 1)
+            share_rows[t, j : j + 1] = jnp.where(here, scores[j : j + 1] / score, 0.0)
+            upright = jnp.sum(jnp.where(row == col, slot, 0.0), axis=1, keepdims=True)
+            source = source + jnp.where(spot == upright, token, 0.0)
+        source = jnp.sum(source, axis=0, keepdims=True).astype(jnp.int32)
+        source_rows[t] = jnp.clip(source, 0, rows - 1)
+
+    build_tables(0, chosen_ref[...], logits_ref[...])
     loads[0].wait()
 
     @pl.loop(0, half)
@@ -132,18 +142,11 @@
             ones, jnp.concatenate([high, low], axis=0), preferred_element_type=jnp.float32
         )
 
-    logits = [logits_ref[j : j + 1] for j in range(TOP)]
-    for j in range(TOP):
-        share_rows[j : j + 1] = logits[j] / sum(logits)
-    tables = [
-        pltpu.make_async_copy(src, dst, route_sem.at[i])
-        for i, (src, dst) in enumerate(
-            ((route_rows, slots), (source_rows, sources), (share_rows, shares))
-        )
+    pl.semaphore_wait(barrier, total - 1)
+    far_copies = [
+        remote(src, dst, far_send.at[i], far_recv.at[i], where_is(mirror))
+        for i, (src, dst) in enumerate(((chosen_ref, far_chosen), (logits_ref, far_logits)))
     ]
-    for copy in tables:
-        copy.start()
-    pl.semaphore_wait(barrier, total - 1)
 
     @pl.loop(1, sp_count)
     def _(i):
@@ -157,6 +160,8 @@
     ).start()
     w_copy = remote(w_hbm, w_buf.at[core], w_sem.at[0], w_sem.at[1], twin)
     w_copy.start()
+    for copy in far_copies:
+        copy.start()
 
     @pl.when(pair == 0)
     def _():
@@ -247,6 +252,17 @@
         pltpu.make_async_copy(crossed.at[i], crossed.at[i], cross_recv.at[i]).wait()
         finish((1 - side) * half + i, crossed[i])
 
+    for copy in far_copies:
+        copy.wait_recv()
+    build_tables(1, far_chosen[...], far_logits[...])
+    tables = [
+        pltpu.make_async_copy(src, dst, route_sem.at[i])
+        for i, (src, dst) in enumerate(
+            ((route_rows, slots), (source_rows, sources), (share_rows, shares))
+        )
+    ]
+    for copy in tables:
+        copy.start()
     lag = jnp.maximum(3, half - 2 * pair)
 
     @pl.loop(0, half)
@@ -314,91 +330,143 @@
     residual = residual.astype(jnp.bfloat16)
     residuals[...] = residual
     inputs = rms_scale(residual.astype(jnp.float32), pre_ref[...]).astype(jnp.bfloat16)
-    segments = D // LANES
-    tokens[...] = inputs.reshape(rows, segments, LANES)
+    piece = D // CHUNKS
+    segments = piece // LANES
+    for c in range(CHUNKS):
+        tokens[c] = inputs[:, c * piece : (c + 1) * piece].reshape(rows, segments, LANES)
     for copy in tables:
         copy.wait()
 
-    def group_of(step):
-        across = lax.rem(plane + step // 2 * 2, PLANES)
-        return across + lax.rem(step, 2) * (1 - 2 * lax.rem(across, 2))
-
-    def block(ref, peer):
-        return ref.at[peer]
-
-    @pl.loop(0, total)
-    def _(i):
-        group = group_of(lax.rem(i // per + 2, PLANES))
-        peer = group * per + lax.rem(place + lax.rem(i, per), per)
-        for r in range(cap):
-            outgoing[peer, r] = tokens[jnp.clip(sources[0, peer * cap + r], 0, rows - 1)]
-
-        @pl.when(peer != me)
+    def neighbour(i):
+        first = lax.rem(place // per + 1 + i // per, 2)
+        return first * per + lax.rem(place + lax.rem(i, per), per)
+
+    def exchange(src, dst, send, recv, peer):
+        where = side_half * near + peer
+
+        @pl.when(peer != place)
         def _():
+            remote(src.at[peer], dst.at[place], send, recv, where_is(where)).start()
+
+        @pl.when(peer == place)
+        def _():
+            pltpu.make_async_copy(src.at[place], dst.at[place], recv).start()
+
+    def dispatch(t, c, start, stop):
+        @pl.loop(start, stop)
+        def _(i):
+            peer = neighbour(i)
+            for r in range(cap):
+                source = jnp.clip(sources[t, 0, peer * cap + r], 0, rows - 1)
+                outgoing[t, c, peer, r] = far_tokens[c][source] if t else tokens[c, source]
+            exchange(outgoing.at[t, c], arrivals.at[t, c], row_send, row_recv.at[t, c], peer)
+
+    def send_tokens():
+        for c in range(CHUNKS):
             remote(
-                block(outgoing, peer), block(arrivals, me), row_send, row_recv.at[plane],
-                where_is(peer),
+                tokens.at[c], far_tokens[c], token_send, token_recv.at[c], where_is(mirror)
             ).start()
 
-        @pl.when(peer == me)
-        def _():
-            pltpu.make_async_copy(
-                block(outgoing, me), block(arrivals, me), row_recv.at[plane]
-            ).start()
+    inner = side_half + place // per == 1
+
+    @pl.when(inner)
+    def _():
+        send_tokens()
+
+    for c in range(CHUNKS):
+        dispatch(0, c, 0, per)
+
+    @pl.when(jnp.logical_not(inner))
+    def _():
+        send_tokens()
+
+    for c in range(CHUNKS):
+        dispatch(0, c, per, near)
+
+    def await_rows(t, c):
+        pltpu.make_async_copy(arrivals.at[t, c], arrivals.at[t, c], row_recv.at[t, c]).wait()
+
+    def answer(t, c):
+        @pl.loop(0, near)
+        def _(i):
+            exchange(
+                results.at[t, c], returned[t][c], back_send, back_recv.at[t, c], neighbour(i)
+            )
+
+    def expert_rows(t):
+        gate_part, up_part = None, None
+        for c in range(CHUNKS):
+            await_rows(t, c)
+            x = arrivals[t, c].reshape(near * cap, piece)
+            cut = slice(c * piece, (c + 1) * piece)
+            g = jnp.dot(x, gate_w[cut, :], preferred_element_type=jnp.float32)
+            u = jnp.dot(x, up_w[cut, :], preferred_element_type=jnp.float32)
+            gate_part = g if c == 0 else gate_part + g
+            up_part = u if c == 0 else up_part + u
+        hidden = (jax.nn.silu(gate_part) * up_part).astype(jnp.bfloat16)
+        for c in range(CHUNKS):
+            result = jnp.dot(
+                hidden, down_w[:, c * piece : (c + 1) * piece], preferred_element_type=jnp.float32
+            )
+            results[t, c] = result.astype(jnp.bfloat16).reshape(near, cap, segments, LANES)
+            if t == 1:
+                answer(t, c)
+
+    def token_sums(t, c, store):
+        pltpu.make_async_copy(returned[t][c], returned[t][c], back_recv.at[t, c]).wait()
+
+        @pl.loop(0, rows // 8)
+        def _(i):
+            for k in range(8):
+                at = i * 8 + k
+                parts = [
+                    returned[t][c][
+                        jnp.clip(slots[t, j, at], 0, near - 1),
+                        jnp.clip(slots[t, TOP + j, at], 0, cap - 1),
+                    ].astype(jnp.float32) * shares[t, j, at]
+                    for j in range(TOP)
+                ]
+                store(at, sum(parts))
 
     for copy in weights:
         copy.wait()
-
-    @pl.loop(0, PLANES)
-    def _(step):
-        group = group_of(step)
-        base = group * per
-        batch = pl.ds(base, per)
-        pltpu.make_async_copy(arrivals.at[batch], arrivals.at[batch], row_recv.at[group]).wait()
-        x = arrivals[batch].reshape(per * cap, D)
-        gate_part = jnp.dot(x, gate_w[...], preferred_element_type=jnp.float32)
-        up_part = jnp.dot(x, up_w[...], preferred_element_type=jnp.float32)
-        hidden = (jax.nn.silu(gate_part) * up_part).astype(jnp.bfloat16)
-        result = jnp.dot(hidden, down_w[...], preferred_element_type=jnp.float32)
-        results[batch] = result.astype(jnp.bfloat16).reshape(per, cap, segments, LANES)
-
-        @pl.loop(0, per)
-        def _(j):
-            peer = base + lax.rem(place + j, per)
-
-            @pl.when(peer != me)
-            def _():
-                remote(
-                    block(results, peer), block(returned, me), back_send, back_recv,
-                    where_is(peer),
-                ).start()
-
-            @pl.when(peer == me)
-            def _():
-                pltpu.make_async_copy(
-                    block(results, me), block(returned, me), back_recv
-                ).start()
-
-    pltpu.make_async_copy(returned, returned, back_recv).wait()
-
-    @pl.loop(0, rows // 8)
-    def _(i):
-        for t in range(8):
-            at = i * 8 + t
-            rows_of = [
-                returned[
-                    jnp.clip(slots[j, at], 0, total - 1), jnp.clip(slots[TOP + j, at], 0, cap - 1)
-                ].astype(jnp.float32)
-                for j in range(TOP)
-            ]
-            combined[at] = rows_of[0] * shares[0, at] + rows_of[1] * shares[1, at]
-
-    routed = rms_scale(combined[...].reshape(rows, D), post_ref[...])
+    for c in range(CHUNKS):
+        pltpu.make_async_copy(far_tokens[c], far_tokens[c], token_recv.at[c]).wait()
+        dispatch(1, c, 0, near)
+        if c == CHUNKS // 2 - 1:
+            expert_rows(0)
+    expert_rows(1)
+    for c in range(CHUNKS):
+        answer(0, c)
+    for c in range(CHUNKS):
+        def store_far(at, value, c=c):
+            sums_out[c, at] = value.astype(jnp.bfloat16)
+
+        token_sums(1, c, store_far)
+        remote(
+            sums_out.at[c], sums_in.at[c], sum_send, sum_recv.at[c], where_is(mirror)
+        ).start()
+    for c in range(CHUNKS):
+        def store_own(at, value, c=c):
+            combined[c, at] = value
+
+        token_sums(0, c, store_own)
+    whole = []
+    for c in range(CHUNKS):
+        pltpu.make_async_copy(sums_in.at[c], sums_in.at[c], sum_recv.at[c]).wait()
+        value = combined[c] + sums_in[c].astype(jnp.float32)
+        whole.append(value.reshape(rows, piece))
+    routed = rms_scale(jnp.concatenate(whole, axis=1), post_ref[...])
     out_ref[...] = (residuals[...].astype(jnp.float32) + routed).astype(jnp.bfloat16)
 
-    others = pl.ds(0, total - 1)
-    pltpu.make_async_copy(outgoing.at[others], outgoing.at[others], row_send).wait()
-    pltpu.make_async_copy(results.at[others], results.at[others], back_send).wait()
+    for copy in far_copies:
+        copy.wait_send()
+    pltpu.make_async_copy(tokens, tokens, token_send).wait()
+    pltpu.make_async_copy(sums_out, sums_out, sum_send).wait()
+    others = pl.ds(0, near - 1)
+    for ref, sem in ((outgoing, row_send), (results, back_send)):
+        done = ref.at[:, :, others]
+        pltpu.make_async_copy(done, done, sem).wait()
 
     sent = extras.at[pl.ds(0, sp_count - 1)]
     pltpu.make_async_copy(sent, sent, extra_send).wait()
@@ -432,8 +500,12 @@
     vmem = pl.BlockSpec(memory_space=pltpu.VMEM)
     anywhere = pl.BlockSpec(memory_space=pl.ANY)
     state = (DV, KEY_WIDTH)
-    table = (1, -(-total * cap // LANES) * LANES)
-    units = pltpu.VMEM((total, cap, D // LANES, LANES), bf16)
+    near = total // 2
+    table = (2, 1, -(-near * cap // LANES) * LANES)
+    segments = D // CHUNKS // LANES
+    units = pltpu.VMEM((2, CHUNKS, near, cap, segments, LANES), bf16)
+    unit = pltpu.VMEM((near, cap, segments, LANES), bf16)
+    sums = pltpu.VMEM((CHUNKS, rows, segments, LANES), bf16)
     dma = pltpu.SemaphoreType.DMA
     return pl.pallas_call(
         layer_kernel,
@@ -467,17 +539,20 @@
             dma((6,)), dma((2,)), dma, dma, dma, dma((half,)), dma, dma((half,)),
             dma, dma((half,)), dma, dma((half,)), dma((ys - 1,)), dma((ys - 1, heads)), dma, dma,
             pltpu.VMEM((rows, D), bf16),
-            pltpu.VMEM((rows, D // LANES, LANES), bf16),
-            units, units, units, units,
-            pltpu.VMEM((rows, D // LANES, LANES), f32),
+            sums, [pltpu.VMEM((rows, segments, LANES), bf16)] * CHUNKS,
+            units, units, units, [[unit] * CHUNKS] * 2, sums, sums,
+            pltpu.VMEM((CHUNKS, rows, segments, LANES), f32),
             *[pltpu.VMEM(w.shape[1:], bf16) for w in (gate_weight, up_weight, down_weight)],
-            pltpu.VMEM((2 * TOP, rows), i32),
+            pltpu.VMEM((TOP, rows), i32),
+            pltpu.VMEM((TOP, rows), f32),
+            pltpu.VMEM((2, 2 * TOP, rows), i32),
             pltpu.VMEM(table, i32),
-            pltpu.VMEM((TOP, rows), f32),
-            pltpu.SMEM((2 * TOP, rows), i32),
+            pltpu.VMEM((2, TOP, rows), f32),
+            pltpu.SMEM((2, 2 * TOP, rows), i32),
             pltpu.SMEM(table, i32),
-            pltpu.SMEM((TOP, rows), f32),
-            dma((3,)), dma((3,)), dma, dma((PLANES,)), dma, dma,
+            pltpu.SMEM((2, TOP, rows), f32),
+            dma((3,)), dma((3,)), dma((2,)), dma((2,)), dma, dma((CHUNKS,)), dma, dma((2, CHUNKS)),
+            dma, dma((2, CHUNKS)), dma, dma((CHUNKS,)),
         ],
         compiler_params=pltpu.CompilerParams(
             collective_id=0, has_side_effects=True, vmem_limit_bytes=60 * 1024 * 1024

time: 134 us -> 126 us (0.940)
  the two profiles are of different devices: /device:TPU:13 before, /device:TPU:0 now
where the time goes in v3:
time: 126 us; the launch traced here: 125 us
  Pallas kernels  123 us (98%)
  local copies, waits for them, and re-layouts  1.88 us (1%)
    pallas_call x1, Pallas kernels, layer(): pl.pallas_call(layer_kernel, in_specs=[anywhere] * 9 + [vmem] * 7, out_sp...  123 us

profile of v3, /device:TPU:0, one launch (start us, length us, event | category | flops | bytes accessed | tf_op | source)
XLA Modules:
  0.0 125.4 jit_solution(12455738692139252142)
XLA Ops:
  0.0 123.5 %layer.1 = bf16[128,2048]{1,0:T(8,128)(2,1)} custom-call(bf16[128,2048]{1,0:T(8,128)(2,1)} %bitcast.19, bf16[128,2048]{1,0:T(8,128)(2,1)} %bitcast.20, bf16[128,4096]{1,0:T(8,128)(2,1)} %bitcast.18, bf16[128,2048]{1,0:T(8,128)(2,1)} %bitcast.21, bf16[128,2048]{1,0:T(8,128)(2,1)} %bitcast.22, bf16[4096,512]{1,0:T(8,128)(2,1)} %w_hbm.1, ...), custom_call_target="tpu_custom_call" | custom-call | tf_op jit(solution)/shard_map/layer/pallas_call | solution.py:510
  123.5 1.9 %copy.18 = bf16[1,128,2048]{2,1,0:T(8,128)(2,1)} copy(bf16[1,128,2048]{2,1,0:T(8,128)(2,1)} %bitcast.17) | data formatting | bytes 1048576

commit v4 on v3

--- a/solution.py
+++ b/solution.py
@@ -24,6 +24,7 @@
 
 
 CHUNKS = 4
+PARTS = 4
 LANES = 128
 MESH = pl.DeviceIdType.MESH
 
@@ -179,6 +180,9 @@
         copy.start()
     pltpu.make_async_copy(extras, extras, extra_recv).wait()
 
+    def state_cut(part):
+        return pl.ds(part * (DV // PARTS), DV // PARTS)
+
     def local_state(h):
         cut = pair_rows(h, KEY_WIDTH)
         extra = jnp.sum(
@@ -212,9 +216,12 @@
             remote(
                 decays_out.at[i], decays.at[side, i], decay_send, decay_recv.at[i], partner
             ).start()
-            remote(
-                states_out.at[i], states.at[side, i], state_send, state_recv.at[i], partner
-            ).start()
+            for part in range(PARTS):
+                cut = state_cut(part)
+                remote(
+                    states_out.at[i, cut], states.at[side, i, cut],
+                    state_send, state_recv.at[i, part], partner,
+                ).start()
 
     @pl.loop(0, half // 2)
     def _(j):
@@ -268,25 +275,34 @@
     @pl.loop(0, half)
     def _(i):
         pltpu.make_async_copy(decays_out.at[i], decays_out.at[i], decay_recv.at[i]).wait()
-        pltpu.make_async_copy(states_out.at[i], states_out.at[i], state_recv.at[i]).wait()
-
-        @pl.when(pair > 0)
-        def _():
-            pltpu.make_async_copy(onward.at[i], onward.at[i], chain_recv.at[i]).wait()
-
-        middle = entering[0, i].astype(jnp.float32) * decays[0, i] + states[0, i].astype(jnp.float32)
-        entering[1, i] = middle.astype(jnp.bfloat16)
-        onward[i] = (middle * decays[1, i] + states[1, i].astype(jnp.float32)).astype(jnp.bfloat16)
-
-        @pl.when(pair < pairs - 1)
-        def _():
+        for part in range(PARTS):
+            cut = state_cut(part)
+            there = states_out.at[i, cut]
+            pltpu.make_async_copy(there, there, state_recv.at[i, part]).wait()
+
+            @pl.when(pair > 0)
+            def _():
+                pltpu.make_async_copy(there, there, chain_recv.at[i, part]).wait()
+
+            middle = entering[0, i, cut].astype(jnp.float32) * decays[0, i] + states[
+                0, i, cut
+            ].astype(jnp.float32)
+            entering[1, i, cut] = middle.astype(jnp.bfloat16)
+            onward[i, cut] = (
+                middle * decays[1, i] + states[1, i, cut].astype(jnp.float32)
+            ).astype(jnp.bfloat16)
+
+            @pl.when(pair < pairs - 1)
+            def _():
+                remote(
+                    onward.at[i, cut], entering.at[0, i, cut],
+                    chain_send, chain_recv.at[i, part], (sp + 2, dp),
+                ).start()
+
             remote(
-                onward.at[i], entering.at[0, i], chain_send, chain_recv.at[i], (sp + 2, dp)
+                entering.at[1 - side, i, cut], crossed.at[i, cut],
+                cross_send, cross_recv.at[i], partner,
             ).start()
-
-        remote(
-            entering.at[1 - side, i], crossed.at[i], cross_send, cross_recv.at[i], partner
-        ).start()
         finish(side * half + i, entering[side, i])
 
         @pl.when(i >= lag)
@@ -412,10 +428,11 @@
             if t == 1:
                 answer(t, c)
 
-    def token_sums(t, c, store):
+    def await_sums(t, c):
         pltpu.make_async_copy(returned[t][c], returned[t][c], back_recv.at[t, c]).wait()
 
-        @pl.loop(0, rows // 8)
+    def token_sums(t, c, store, start, stop):
+        @pl.loop(start // 8, stop // 8)
         def _(i):
             for k in range(8):
                 at = i * 8 + k
@@ -436,21 +453,28 @@
         if c == CHUNKS // 2 - 1:
             expert_rows(0)
     expert_rows(1)
-    for c in range(CHUNKS):
+    for c in range(2):
         answer(0, c)
     for c in range(CHUNKS):
         def store_far(at, value, c=c):
             sums_out[c, at] = value.astype(jnp.bfloat16)
 
-        token_sums(1, c, store_far)
-        remote(
-            sums_out.at[c], sums_in.at[c], sum_send, sum_recv.at[c], where_is(mirror)
-        ).start()
+        await_sums(1, c)
+        for start in (0, rows // 2):
+            some = pl.ds(start, rows // 2)
+            token_sums(1, c, store_far, start, start + rows // 2)
+            remote(
+                sums_out.at[c, some], sums_in.at[c, some], sum_send, sum_recv.at[c],
+                where_is(mirror),
+            ).start()
+        if c < CHUNKS - 2:
+            answer(0, c + 2)
     for c in range(CHUNKS):
         def store_own(at, value, c=c):
             combined[c, at] = value
 
-        token_sums(0, c, store_own)
+        await_sums(0, c)
+        token_sums(0, c, store_own, 0, rows)
     whole = []
     for c in range(CHUNKS):
         pltpu.make_async_copy(sums_in.at[c], sums_in.at[c], sum_recv.at[c]).wait()
@@ -536,8 +560,8 @@
             pltpu.VMEM((ys - 1, heads, rows, DV), bf16),
             pltpu.VMEM((ys - 1, rows, 2 * cols), bf16),
             pltpu.VMEM((ys, rows, 2 * cols), bf16),
-            dma((6,)), dma((2,)), dma, dma, dma, dma((half,)), dma, dma((half,)),
-            dma, dma((half,)), dma, dma((half,)), dma((ys - 1,)), dma((ys - 1, heads)), dma, dma,
+            dma((6,)), dma((2,)), dma, dma, dma, dma((half, PARTS)), dma, dma((half,)),
+            dma, dma((half, PARTS)), dma, dma((half,)), dma((ys - 1,)), dma((ys - 1, heads)), dma, dma,
             pltpu.VMEM((rows, D), bf16),
             sums, [pltpu.VMEM((rows, segments, LANES), bf16)] * CHUNKS,
             units, units, units, [[unit] * CHUNKS] * 2, sums, sums,

time: 126 us -> 123 us (0.976)
  the two profiles are of different devices: /device:TPU:0 before, /device:TPU:5 now
where the time goes in v4:
time: 123 us
  Pallas kernels  121 us (98%)
  local copies, waits for them, and re-layouts  1.88 us (2%)
    pallas_call x1, Pallas kernels, layer(): pl.pallas_call(layer_kernel, in_specs=[anywhere] * 9 + [vmem] * 7, out_sp...  121 us

profile of v4, /device:TPU:5, one launch (start us, length us, event | category | flops | bytes accessed | tf_op | source)
XLA Modules:
  0.0 123.2 jit_solution(10564535777609148240)
XLA Ops:
  0.0 121.3 %layer.1 = bf16[128,2048]{1,0:T(8,128)(2,1)} custom-call(bf16[128,2048]{1,0:T(8,128)(2,1)} %bitcast.19, bf16[128,2048]{1,0:T(8,128)(2,1)} %bitcast.20, bf16[128,4096]{1,0:T(8,128)(2,1)} %bitcast.18, bf16[128,2048]{1,0:T(8,128)(2,1)} %bitcast.21, bf16[128,2048]{1,0:T(8,128)(2,1)} %bitcast.22, bf16[4096,512]{1,0:T(8,128)(2,1)} %w_hbm.1, ...), custom_call_target="tpu_custom_call" | custom-call | tf_op jit(solution)/shard_map/layer/pallas_call | solution.py:534
  121.3 1.9 %copy.18 = bf16[1,128,2048]{2,1,0:T(8,128)(2,1)} copy(bf16[1,128,2048]{2,1,0:T(8,128)(2,1)} %bitcast.17) | data formatting | bytes 1048576
